TPU v7x, 32 devices: a whole 2x2x4 slice. The times are simulated.
32 devices in a mesh: grp: 2 (over x), fs: 4 (over z), tp: 4 (over y, core).
Axes of the slice: x: 2, y: 2, z: 4, core: 2. Of those that a mesh axis runs over, the one named last changes fastest.
Arguments:
- stream: bfloat16 [2048, 2048], P(('grp', 'fs'), 'tp'), parts along dimension 0, may hold values from -80 to 80
- mixed: bfloat16 [2048, 2048], P(('grp', 'fs'), 'tp'), parts along dimension 0, may hold values from -6 to 6
- out_weight: bfloat16 [2048, 2048], P('fs', 'tp'), may hold values from -0.125 to 0.125
- norm_gain: bfloat16 [2048], P('tp'), may hold values from 0.099609375 to 1.8984375
- up_weight: bfloat16 [2048, 8192], P('fs', 'tp'), may hold values from -0.125 to 0.125
- down_weight: bfloat16 [8192, 2048], P('tp', 'fs'), may hold values from -0.09375 to 0.09375
Outputs:
- result: bfloat16 [2048, 2048], P(('grp', 'fs'), 'tp'), parts along dimension 0
There are 2 independent parts, one for each index of `grp`. A program takes and returns all parts, laid end to end along the dimension named above; an argument that names none is the same for every part. Nothing has to cross between parts.
All inputs are finite; a program needn't handle non-finite values.
Results may differ from a plain program's by a relative error of at most 0.01.
Values may be sent and summed in bfloat16 or wider, within the bound.
A program may use at most 64 MiB of HBM per device.

v0:
```python
import jax
import jax.numpy as jnp
from jax import lax
from jax.sharding import PartitionSpec as P

epsilon = 1e-06


def fold_product(left, portion):
    return jnp.dot(left, portion, preferred_element_type=jnp.float32)


def body(stream, mixed, out_weight, norm_gain, up_weight, down_weight):
    mixed_whole = lax.all_gather(mixed, "tp", axis=1, tiled=True)
    projected = fold_product(mixed_whole, lax.all_gather(out_weight, "fs", axis=0, tiled=True))
    resid = (stream.astype(jnp.float32) + projected).astype(jnp.bfloat16)
    widened = resid.astype(jnp.float32)
    resid_whole, gain_whole = (
        lax.all_gather(resid, "tp", axis=1, tiled=True),
        lax.all_gather(norm_gain, "tp", axis=0, tiled=True),
    )
    stream_wide = resid_whole.astype(jnp.float32)
    energy = jnp.mean(stream_wide * stream_wide, axis=1, keepdims=True)
    normed_whole = (
        stream_wide * lax.rsqrt(energy + epsilon) * gain_whole.astype(jnp.float32)
    ).astype(jnp.bfloat16)
    up_full = lax.all_gather(up_weight, "fs", axis=0, tiled=True)
    up_values = jnp.dot(normed_whole, up_full, preferred_element_type=jnp.float32)
    activated = jnp.square(jax.nn.relu(up_values)).astype(jnp.bfloat16)
    partials = jnp.dot(
        activated,
        lax.all_gather(down_weight, "fs", axis=1, tiled=True),
        preferred_element_type=jnp.float32,
    )
    branch = lax.psum_scatter(partials, "tp", scatter_dimension=1, tiled=True)
    return (widened + branch).astype(jnp.bfloat16)


def solution(mesh):
    placed = (
        P(("grp", "fs"), "tp"),
        P(("grp", "fs"), "tp"),
        P("fs", "tp"),
        P("tp"),
        P("fs", "tp"),
        P("tp", "fs"),
    )
    return jax.shard_map(
        body, mesh=mesh, in_specs=placed, out_specs=P(("grp", "fs"), "tp"), check_vma=False
    )
```

profile of v0, /device:TPU:1, one launch (start us, length us, event | category | flops | bytes accessed | tf_op | source)
XLA Modules:
  0.0 444.3 jit_solution(17761984811447888567)
XLA Ops:
  6.5 0.0 all-gather.7.cloned.1.call-start
  6.5 0.7 all-gather.7.cloned.1.call-update
  7.3 0.0 all-gather.9.cloned.1.call-start
  7.3 0.7 all-gather.9.cloned.1.call-update
  8.0 0.0 all-gather.11.cloned.1.call-start
  8.1 20.0 %all-gather.7.cloned.1.call-done = bf16[256,2048]{1,0:T(8,128)(2,1)} async-done(((bf16[256,512]{1,0:T(8,128)(2,1)}), bf16[256,2048]{1,0:T(8,128)(2,1)}) %all-gather.7.cloned.1.call-update) | async-done | bytes 1048592 | tf_op jit(solution)/shard_map/all_gather | solution.py:14
  28.1 46.7 %all-gather.9.cloned.1.call-done = bf16[2048,512]{1,0:T(8,128)(2,1)} async-done(((bf16[512,512]{1,0:T(8,128)(2,1)}), bf16[2048,512]{1,0:T(8,128)(2,1)}) %all-gather.9.cloned.1.call-update) | async-done | bytes 2097168 | tf_op jit(solution)/shard_map/all_gather | solution.py:15
  74.8 3.3 fusion.5
  78.1 0.0 all-gather.11.cloned.1.call-update
  78.1 0.0 copy-start.1
  78.1 0.0 all-gather.13.cloned.1.call-start
  78.2 0.5 all-gather.13.cloned.1.call-update
  78.7 0.0 all-gather.15.cloned.1.call-start
  78.8 0.5 all-gather.15.cloned.1.call-update
  79.3 0.0 reduce-scatter.2.cloned.1.call-start
  79.3 0.0 copy-done.1
  79.4 5.9 %all-gather = bf16[4,1,512]{2,1,0:T(2,128)(2,1)S(1)} all-gather(bf16[1,1,512]{2,1,0:T(2,128)(2,1)S(1)} %reshape.9), channel_id=1, replica_groups=mesh['grp'=2,'fs'=4,'tp'=4] {'tp'}, dimensions={0}, use_global_device_ids=true | all-gather | bytes 5120 | tf_op jit(solution)/shard_map/all_gather | solution.py:20
  85.2 9.1 %all-gather.11.cloned.1.call-done = bf16[256,2048]{1,0:T(8,128)(2,1)} async-done(((bf16[256,512]{1,0:T(8,128)(2,1)}), bf16[256,2048]{1,0:T(8,128)(2,1)}) %all-gather.11.cloned.1.call-update) | async-done | bytes 1048592 | tf_op jit(solution)/shard_map/all_gather | solution.py:19
  94.3 1.5 fusion.2
  95.9 149.3 %all-gather.13.cloned.1.call-done = bf16[2048,2048]{1,0:T(8,128)(2,1)} async-done(((bf16[512,2048]{1,0:T(8,128)(2,1)}), bf16[2048,2048]{1,0:T(8,128)(2,1)}) %all-gather.13.cloned.1.call-update) | async-done | bytes 8388624 | tf_op jit(solution)/shard_map/all_gather | solution.py:27
  245.2 149.2 %all-gather.15.cloned.1.call-done = bf16[2048,2048]{1,0:T(8,128)(2,1)} async-done(((bf16[2048,512]{1,0:T(8,128)(2,1)}), bf16[2048,2048]{1,0:T(8,128)(2,1)}) %all-gather.15.cloned.1.call-update) | async-done | bytes 8388624 | tf_op jit(solution)/shard_map/all_gather | solution.py:32
  394.4 11.9 %fusion.10 = f32[256,2048]{1,0:T(8,128)} fusion(bf16[2048,2048]{1,0:T(8,128)(2,1)} %all-gather.15.cloned.1.call-done, bf16[2048,2048]{1,0:T(8,128)(2,1)} %all-gather.13.cloned.1.call-done, bf16[256,2048]{1,0:T(8,128)(2,1)} %all-gather.11.cloned.1.call-done, f32[2048]{0:T(1024)S(1)} %bitcast.5, f32[256]{0:T(256)S(1)} %add_rsqrt_fusion), kind=kOutput, calls=%fused_computation.12 | convolution fusion | flops 4298637312 | bytes 19932160 | tf_op jit(solution)/shard_map/dot_general | solution.py:30
  406.4 0.0 copy-start
  406.4 0.0 reduce-scatter.2.cloned.1.call-update
  406.4 29.2 %reduce-scatter.2.cloned.1.call-done = f32[256,512]{1,0:T(8,128)} async-done(((f32[256,2048]{1,0:T(8,128)}), f32[256,512]{1,0:T(8,128)}) %reduce-scatter.2.cloned.1.call-update) | async-done | bytes 524304 | tf_op jit(solution)/shard_map/reduce_scatter | solution.py:35
  435.6 0.0 copy-done
  435.6 1.8 add_convert_fusion
  (3 shorter events, 0.0 us)
Async XLA Ops:
  6.5 21.5 %all-gather.7.cloned.1.call-start = ((), (), s32[]{:S(2)}) async-start(), calls=%async_computation.1 | async-start | bytes 1310720 | tf_op jit(solution)/shard_map/all_gather | solution.py:14
  7.3 67.5 %all-gather.9.cloned.1.call-start = ((), (), s32[]{:S(2)}) async-start(), calls=%async_computation.2 | async-start | bytes 2621440 | tf_op jit(solution)/shard_map/all_gather | solution.py:15
  8.0 86.3 %all-gather.11.cloned.1.call-start = ((), (), s32[]{:S(2)}) async-start(), calls=%async_computation.3 | async-start | bytes 1310720 | tf_op jit(solution)/shard_map/all_gather | solution.py:19
  78.1 1.2 copy-start.1
  78.1 167.1 %all-gather.13.cloned.1.call-start = ((), (), s32[]{:S(2)}) async-start(), calls=%async_computation.4 | async-start | bytes 10485760 | tf_op jit(solution)/shard_map/all_gather | solution.py:27
  78.7 315.7 %all-gather.15.cloned.1.call-start = ((), (), s32[]{:S(2)}) async-start(), calls=%async_computation.5 | async-start | bytes 10485760 | tf_op jit(solution)/shard_map/all_gather | solution.py:32
  79.3 356.3 %reduce-scatter.2.cloned.1.call-start = ((), (), s32[]{:S(2)}) async-start(), calls=%async_computation.6 | async-start | bytes 2621440 | tf_op jit(solution)/shard_map/reduce_scatter | solution.py:35
  406.4 29.2 %copy-start = (bf16[256,512]{1,0:T(8,128)(2,1)S(1)}, bf16[256,512]{1,0:T(8,128)(2,1)}, u32[]{:S(2)}) copy-start(bf16[256,512]{1,0:T(8,128)(2,1)} %fusion.5) | copy-start | bytes 786436
Sparse Core Ops, SparseCore 0:
  8.9 19.1 all-gather.6
  29.6 45.0 all-gather.8
  78.2 16.0 all-gather.10
  95.8 149.3 all-gather.12
  246.6 147.7 all-gather.14
  406.5 29.0 reduce-scatter.1
where the time goes:
time: 445 us; the launch traced here: 444 us
  waiting for transfers between devices  406 us (91%)
  matrix products  15.3 us (3%)
  between operations  13.5 us (3%)
  blocking collectives  5.86 us (1%)
    all_gather x1, waiting for transfers between devices, body(): up_full = lax.all_gather(up_weight, 'fs', axis=0, tiled=True)  149 us
    all_gather x1, waiting for transfers between devices, body(): lax.all_gather(down_weight, 'fs', axis=1, tiled=True)  149 us
    all_gather x1, waiting for transfers between devices, body(): lax.all_gather(out_weight, 'fs', axis=0, tiled=True)  46.7 us
    reduce_scatter x1, waiting for transfers between devices, body(): branch = lax.psum_scatter(partials, 'tp', scatter_dimension=1, tiled=True)  29.2 us
    all_gather x1, waiting for transfers between devices, body(): mixed_whole = lax.all_gather(mixed, 'tp', axis=1, tiled=True)  20 us
    dot_general x1, matrix products, body(): jnp.dot(activated, lax.all_gather(down_weight, 'fs', axis=1, tiled=True),...  11.9 us
    all_gather x1, waiting for transfers between devices, body(): lax.all_gather(resid, 'tp', axis=1, tiled=True)  9.09 us
  transfers between devices with their start and end apart: 6, of which 6 were waited for; matrix products, arithmetic and copies ran while one was open for 0% of the time, Pallas kernels for 0%

commit v1 on v0

--- a/solution.py
+++ b/solution.py
@@ -10,7 +10,7 @@
     return jnp.dot(left, portion, preferred_element_type=jnp.float32)
 
 
-def body(stream, mixed, out_weight, norm_gain, up_weight, down_weight):
+def gathered_body(stream, mixed, out_weight, norm_gain, up_weight, down_weight):
     mixed_whole = lax.all_gather(mixed, "tp", axis=1, tiled=True)
     projected = fold_product(mixed_whole, lax.all_gather(out_weight, "fs", axis=0, tiled=True))
     resid = (stream.astype(jnp.float32) + projected).astype(jnp.bfloat16)
@@ -36,6 +36,26 @@
     return (widened + branch).astype(jnp.bfloat16)
 
 
+def spread_body(stream, mixed, out_weight, norm_gain, up_weight, down_weight):
+    mixed_whole = lax.all_gather(mixed, "tp", axis=1, tiled=True)
+    out_full = lax.all_gather(out_weight, "fs", axis=0, tiled=True)
+    up_mine = lax.all_to_all(up_weight, "fs", split_axis=1, concat_axis=0, tiled=True)
+    down_mine = lax.all_to_all(down_weight, "fs", split_axis=0, concat_axis=1, tiled=True)
+    projected = jnp.dot(mixed_whole, out_full, preferred_element_type=jnp.float32)
+    resid = (stream.astype(jnp.float32) + projected).astype(jnp.bfloat16)
+    rows = lax.all_gather(resid, "fs", axis=0, tiled=True)
+    whole = lax.all_gather(rows, "tp", axis=1, tiled=True).astype(jnp.float32)
+    gain = lax.all_gather(norm_gain, "tp", axis=0, tiled=True).astype(jnp.float32)
+    energy = jnp.mean(whole * whole, axis=1, keepdims=True)
+    normed = (whole * lax.rsqrt(energy + epsilon) * gain).astype(jnp.bfloat16)
+    up_values = jnp.dot(normed, up_mine, preferred_element_type=jnp.float32)
+    activated = jnp.square(jax.nn.relu(up_values)).astype(jnp.bfloat16)
+    partials = jnp.dot(activated, down_mine, preferred_element_type=jnp.float32).astype(jnp.bfloat16)
+    columns = lax.psum_scatter(partials, "tp", scatter_dimension=1, tiled=True)
+    branch = lax.psum_scatter(columns, "fs", scatter_dimension=0, tiled=True)
+    return (resid.astype(jnp.float32) + branch.astype(jnp.float32)).astype(jnp.bfloat16)
+
+
 def solution(mesh):
     placed = (
         P(("grp", "fs"), "tp"),
@@ -45,6 +65,19 @@
         P("fs", "tp"),
         P("tp", "fs"),
     )
-    return jax.shard_map(
-        body, mesh=mesh, in_specs=placed, out_specs=P(("grp", "fs"), "tp"), check_vma=False
-    )
+    fs, tp = mesh.shape["fs"], mesh.shape["tp"]
+
+    def call(stream, mixed, out_weight, norm_gain, up_weight, down_weight):
+        width, hidden = up_weight.shape
+        tokens = stream.shape[0] // mesh.shape["grp"]
+        moved_weights = 2 * width * hidden // tp
+        moved_rows = 2 * tokens * width + 2 * width * hidden // (tp * fs)
+        body = spread_body if moved_rows < moved_weights else gathered_body
+        return sharded(body)(stream, mixed, out_weight, norm_gain, up_weight, down_weight)
+
+    def sharded(body):
+        return jax.shard_map(
+            body, mesh=mesh, in_specs=placed, out_specs=P(("grp", "fs"), "tp"), check_vma=False
+        )
+
+    return call

time: 445 us -> 299 us (0.67)
  waiting for transfers between devices: 406 us -> 241 us
  local copies, waits for them, and re-layouts: 0.01 us -> 10.6 us
  starting transfers between devices: 0.2 us -> 8.42 us
    all_gather x5 -> x4, waiting for transfers between devices: 374 us -> 108 us  [the longest x1 46.7 us: spread_body(): out_full = lax.all_gather(out_weight, 'fs', axis=0, tiled=True)]
    all_to_all x0 -> x2, waiting for transfers between devices: none -> 57.8 us  [the longest x1 38.7 us: spread_body(): lax.all_to_all(up_weight, 'fs', split_axis=1, concat_axis=0, tiled=True)]
    reduce_scatter x1 -> x2, waiting for transfers between devices: 29.2 us -> 73.3 us  [the longest x1 44.1 us: spread_body(): columns = lax.psum_scatter(partials, 'tp', scatter_dimension=1, tiled=True)]
    all_to_all x0 -> x2, starting transfers between devices: none -> 8.21 us  [the longest x1 4.59 us: spread_body(): lax.all_to_all(up_weight, 'fs', split_axis=1, concat_axis=0, tiled=True)]
    all_to_all x0 -> x2, local copies, waits for them, and re-layouts: none -> 6.6 us  [the longest x1 4.2 us: spread_body(): lax.all_to_all(up_weight, 'fs', split_axis=1, concat_axis=0, tiled=True)]
  transfers between devices with their start and end apart: 6 -> 8, of which waited for: 6 -> 7; matrix products, arithmetic and copies ran while one was open for 0% -> 4% of each run, Pallas kernels for 0% -> 0%
where the time goes in v1:
time: 299 us; the launch traced here: 298 us
  waiting for transfers between devices  241 us (81%)
  between operations  13.5 us (5%)
  matrix products  12.7 us (4%)
  local copies, waits for them, and re-layouts  10.6 us (4%)
  starting transfers between devices  8.42 us (3%)
  blocking collectives  6.6 us (2%)
  other arithmetic  4.95 us (2%)
    all_gather x1, waiting for transfers between devices, spread_body(): out_full = lax.all_gather(out_weight, 'fs', axis=0, tiled=True)  46.7 us
    reduce_scatter x1, waiting for transfers between devices, spread_body(): columns = lax.psum_scatter(partials, 'tp', scatter_dimension=1, tiled=True)  44.1 us
    all_gather x1, waiting for transfers between devices, spread_body(): rows = lax.all_gather(resid, 'fs', axis=0, tiled=True)  41.5 us
    all_to_all x1, waiting for transfers between devices, spread_body(): lax.all_to_all(up_weight, 'fs', split_axis=1, concat_axis=0, tiled=True)  38.7 us
    reduce_scatter x1, waiting for transfers between devices, spread_body(): branch = lax.psum_scatter(columns, 'fs', scatter_dimension=0, tiled=True)  29.2 us
    all_gather x1, waiting for transfers between devices, spread_body(): mixed_whole = lax.all_gather(mixed, 'tp', axis=1, tiled=True)  20 us
    all_to_all x1, waiting for transfers between devices, spread_body(): lax.all_to_all(down_weight, 'fs', split_axis=0, concat_axis=1, tiled=True)  19.1 us
    dot_general x1, matrix products, spread_body(): jnp.dot(activated, down_mine, preferred_element_type=jnp.float32)  9.4 us
  transfers between devices with their start and end apart: 8, of which 7 were waited for; matrix products, arithmetic and copies ran while one was open for 4% of the time, Pallas kernels for 0%

profile of v1, /device:TPU:1, one launch (start us, length us, event | category | flops | bytes accessed | tf_op | source)
XLA Modules:
  0.0 297.6 jit_solution(17435808376531385950)
XLA Ops:
  6.5 0.0 all-gather.6.cloned.1.call-start
  6.5 0.7 all-gather.6.cloned.1.call-update
  7.3 0.0 all-gather.8.cloned.1.call-start
  7.3 0.7 all-gather.8.cloned.1.call-update
  8.0 0.0 all-gather.10.cloned.1.call-start
  8.1 20.0 %all-gather.6.cloned.1.call-done = bf16[256,2048]{1,0:T(8,128)(2,1)} async-done(((bf16[256,512]{1,0:T(8,128)(2,1)}), bf16[256,2048]{1,0:T(8,128)(2,1)}) %all-gather.6.cloned.1.call-update) | async-done | bytes 1048592 | tf_op jit(solution)/shard_map/all_gather | solution.py:40
  28.1 46.7 %all-gather.8.cloned.1.call-done = bf16[2048,512]{1,0:T(8,128)(2,1)} async-done(((bf16[512,512]{1,0:T(8,128)(2,1)}), bf16[2048,512]{1,0:T(8,128)(2,1)}) %all-gather.8.cloned.1.call-update) | async-done | bytes 2097168 | tf_op jit(solution)/shard_map/all_gather | solution.py:41
  74.8 3.3 %fusion.9 = bf16[256,512]{1,0:T(8,128)(2,1)} fusion(bf16[256,2048]{1,0:T(8,128)(2,1)} %all-gather.6.cloned.1.call-done, bf16[2048,512]{1,0:T(8,128)(2,1)} %all-gather.8.cloned.1.call-done, bf16[256,512]{1,0:T(8,128)(2,1)} %param.6), kind=kOutput, calls=%fused_computation.11 | convolution fusion | flops 537264128 | bytes 3670016 | tf_op jit(solution)/shard_map/dot_general | solution.py:44
  78.1 0.0 all-gather.10.cloned.1.call-update
  78.1 3.6 %all-to-all-start.1 = ((bf16[4,512,512]{2,1,0:T(8,128)(2,1)}), bf16[4,512,512]{2,1,0:T(8,128)(2,1)S(1)}, u32[]{:S(2)}, u32[]{:S(2)}) async-start(bf16[4,512,512]{2,1,0:T(8,128)(2,1)} %bitcast.13), calls=%async_computation.1 | async-start | bytes 4194304 | tf_op jit(solution)/shard_map/all_to_all | solution.py:43
  81.7 0.0 all-gather.12.cloned.1.call-start
  81.8 41.5 %all-gather.10.cloned.1.call-done = bf16[1024,512]{1,0:T(8,128)(2,1)} async-done(((bf16[256,512]{1,0:T(8,128)(2,1)}), bf16[1024,512]{1,0:T(8,128)(2,1)}) %all-gather.10.cloned.1.call-update) | async-done | bytes 1048592 | tf_op jit(solution)/shard_map/all_gather | solution.py:46
  123.3 0.0 all-gather.12.cloned.1.call-update
  123.3 4.0 %copy.10 = bf16[512,2048]{0,1:T(8,128)(2,1)} copy(bf16[512,2048]{1,0:T(8,128)(2,1)} %param.10) | data formatting | bytes 4194304 | tf_op args[4]
  127.3 19.1 %all-to-all-done.1 = bf16[4,512,512]{2,1,0:T(8,128)(2,1)S(1)} async-done(((bf16[4,512,512]{2,1,0:T(8,128)(2,1)}), bf16[4,512,512]{2,1,0:T(8,128)(2,1)S(1)}, u32[]{:S(2)}, u32[]{:S(2)}) %all-to-all-start.1) | async-done | bytes 2097184 | tf_op jit(solution)/shard_map/all_to_all | solution.py:43
  146.3 0.0 copy-start.2
  146.3 4.6 %all-to-all-start = ((bf16[512,4,512]{0,2,1:T(8,128)(2,1)}), bf16[512,4,512]{0,2,1:T(8,128)(2,1)}, u32[]{:S(2)}, u32[]{:S(2)}) async-start(bf16[512,4,512]{0,2,1:T(8,128)(2,1)} %bitcast.12), calls=%async_computation | async-start | bytes 4194304 | tf_op jit(solution)/shard_map/all_to_all | solution.py:42
  150.9 0.0 reduce-scatter.3.cloned.1.call-start
  151.0 0.0 copy-done.2
  151.0 6.6 %all-gather = bf16[4,1,512]{2,1,0:T(2,128)(2,1)S(1)} all-gather(bf16[1,1,512]{2,1,0:T(2,128)(2,1)S(1)} %reshape.15), channel_id=1, replica_groups=mesh['grp'=2,'fs'=4,'tp'=4] {'tp'}, dimensions={0}, use_global_device_ids=true | all-gather | bytes 5120 | tf_op jit(solution)/shard_map/all_gather | solution.py:48
  157.6 2.4 copy.12
  160.0 38.7 %all-to-all-done = bf16[512,4,512]{0,2,1:T(8,128)(2,1)} async-done(((bf16[512,4,512]{0,2,1:T(8,128)(2,1)}), bf16[512,4,512]{0,2,1:T(8,128)(2,1)}, u32[]{:S(2)}, u32[]{:S(2)}) %all-to-all-start) | async-done | bytes 2097184 | tf_op jit(solution)/shard_map/all_to_all | solution.py:42
  198.7 4.2 %copy.11 = bf16[4,512,512]{2,1,0:T(8,128)(2,1)} copy(bf16[4,512,512]{1,2,0:T(8,128)(2,1)} %bitcast.2) | data formatting | bytes 4194304 | tf_op jit(solution)/shard_map/all_to_all | solution.py:42
  202.9 0.0 copy-start
  202.9 0.0 all-gather.12.cloned.1.call-done
  202.9 3.2 %fusion = f32[1024]{0:T(1024)S(1)} fusion(bf16[1024,2048]{1,0:T(8,128)(2,1)} %all-gather.12.cloned.1.call-done), kind=kLoop, calls=%fused_computation.2 | loop fusion | flops 6290432 | bytes 4198400 | tf_op jit(solution)/shard_map/reduce_sum | solution.py:49
  206.2 0.0 copy-done
  206.2 9.4 %convolution_convert_fusion = bf16[1024,2048]{1,0:T(8,128)(2,1)} fusion(bf16[512,2048]{0,1:T(8,128)(2,1)S(1)} %bitcast.14, bf16[2048,512]{1,0:T(8,128)(2,1)} %bitcast.15, bf16[1024,2048]{1,0:T(8,128)(2,1)} %all-gather.12.cloned.1.call-done, f32[2048]{0:T(1024)S(1)} %bitcast.16, f32[1024]{0:T(1024)S(1)} %add_rsqrt_fusion), kind=kOutput, calls=%fused_computation.8 | convolution fusion | flops 4307025920 | bytes 12595200 | tf_op jit(solution)/shard_map/dot_general | solution.py:53
  215.6 0.0 copy-start.1
  215.6 0.0 reduce-scatter.3.cloned.1.call-update
  215.6 0.0 reduce-scatter.5.cloned.1.call-start
  215.6 44.1 %reduce-scatter.3.cloned.1.call-done = bf16[1024,512]{1,0:T(8,128)(2,1)} async-done(((bf16[1024,2048]{1,0:T(8,128)(2,1)}), bf16[1024,512]{1,0:T(8,128)(2,1)}) %reduce-scatter.3.cloned.1.call-update) | async-done | bytes 1048592 | tf_op jit(solution)/shard_map/reduce_scatter | solution.py:54
  259.8 0.0 reduce-scatter.5.cloned.1.call-update
  259.8 29.2 %reduce-scatter.5.cloned.1.call-done = bf16[256,512]{1,0:T(8,128)(2,1)} async-done(((bf16[1024,512]{1,0:T(8,128)(2,1)}), bf16[256,512]{1,0:T(8,128)(2,1)}) %reduce-scatter.5.cloned.1.call-update) | async-done | bytes 262160 | tf_op jit(solution)/shard_map/reduce_scatter | solution.py:55
  289.0 0.0 copy-done.1
  289.0 1.7 add_convert_fusion
  (3 shorter events, 0.0 us)
Async XLA Ops:
  6.5 21.5 %all-gather.6.cloned.1.call-start = ((), (), s32[]{:S(2)}) async-start(), calls=%async_computation.4 | async-start | bytes 1310720 | tf_op jit(solution)/shard_map/all_gather | solution.py:40
  7.3 67.5 %all-gather.8.cloned.1.call-start = ((), (), s32[]{:S(2)}) async-start(), calls=%async_computation.5 | async-start | bytes 2621440 | tf_op jit(solution)/shard_map/all_gather | solution.py:41
  8.0 115.3 %all-gather.10.cloned.1.call-start = ((), (), s32[]{:S(2)}) async-start(), calls=%async_computation.6 | async-start | bytes 1310720 | tf_op jit(solution)/shard_map/all_gather | solution.py:46
  78.1 68.2 %all-to-all-start.1 = ((bf16[4,512,512]{2,1,0:T(8,128)(2,1)}), bf16[4,512,512]{2,1,0:T(8,128)(2,1)S(1)}, u32[]{:S(2)}, u32[]{:S(2)}) async-start(bf16[4,512,512]{2,1,0:T(8,128)(2,1)} %bitcast.13), calls=%async_computation.1 | async-start | bytes 4194304 | tf_op jit(solution)/shard_map/all_to_all | solution.py:43
  81.7 121.2 %all-gather.12.cloned.1.call-start = ((), (), s32[]{:S(2)}) async-start(), calls=%async_computation.7 | async-start | bytes 5242880 | tf_op jit(solution)/shard_map/all_gather | solution.py:47
  146.3 4.7 %copy-start.2 = (bf16[512]{0:T(512)(128)(2,1)S(1)}, bf16[512]{0:T(512)(128)(2,1)}, u32[]{:S(2)}) copy-start(bf16[512]{0:T(512)(128)(2,1)} %param.9) | copy-start | bytes 3076
  146.3 52.4 %all-to-all-start = ((bf16[512,4,512]{0,2,1:T(8,128)(2,1)}), bf16[512,4,512]{0,2,1:T(8,128)(2,1)}, u32[]{:S(2)}, u32[]{:S(2)}) async-start(bf16[512,4,512]{0,2,1:T(8,128)(2,1)} %bitcast.12), calls=%async_computation | async-start | bytes 4194304 | tf_op jit(solution)/shard_map/all_to_all | solution.py:42
  150.9 108.8 %reduce-scatter.3.cloned.1.call-start = ((), (), s32[]{:S(2)}) async-start(), calls=%async_computation.8 | async-start | bytes 5242880 | tf_op jit(solution)/shard_map/reduce_scatter | solution.py:54
  202.9 3.2 %copy-start = (bf16[512,4,512]{0,2,1:T(8,128)(2,1)S(1)}, bf16[512,4,512]{0,2,1:T(8,128)(2,1)}, u32[]{:S(2)}) copy-start(bf16[512,4,512]{0,2,1:T(8,128)(2,1)} %copy.12) | copy-start | bytes 6291460
  215.6 73.4 %copy-start.1 = (bf16[256,512]{1,0:T(8,128)(2,1)S(1)}, bf16[256,512]{1,0:T(8,128)(2,1)}, u32[]{:S(2)}) copy-start(bf16[256,512]{1,0:T(8,128)(2,1)} %fusion.9) | copy-start | bytes 786436
  215.6 73.4 %reduce-scatter.5.cloned.1.call-start = ((), (), s32[]{:S(2)}) async-start(), calls=%async_computation.9 | async-start | bytes 1310720 | tf_op jit(solution)/shard_map/reduce_scatter | solution.py:55
Sparse Core Ops, SparseCore 0:
  8.9 19.1 all-gather.5
  29.6 45.0 all-gather.7
  78.2 44.9 all-gather.9
  124.7 47.4 all-gather.11
  215.7 43.9 reduce-scatter.2
  261.9 27.0 reduce-scatter.4

commit v2 on v1

--- a/solution.py
+++ b/solution.py
@@ -1,6 +1,10 @@
+import functools
+
 import jax
 import jax.numpy as jnp
 from jax import lax
+from jax.experimental import pallas as pl
+from jax.experimental.pallas import tpu as pltpu
 from jax.sharding import PartitionSpec as P
 
 epsilon = 1e-06
@@ -56,6 +60,235 @@
     return (resid.astype(jnp.float32) + branch.astype(jnp.float32)).astype(jnp.bfloat16)
 
 
+MESH = pl.DeviceIdType.MESH
+
+
+def slot_table(fs):
+    table, count = {}, 0
+    sizes = dict(
+        mixed=3, gain=3, out_z=fs, out_x=fs, up_z=fs, up_x=fs, down_z=fs, down_x=fs,
+        rows_z=fs, rows_y=fs, rows_c=fs, rows_d=fs, sum_c=fs, sum_y=fs, sum_z=fs, own=fs,
+    )
+    for name, size in sizes.items():
+        table[name] = count
+        count += size
+    return table, count
+
+
+def layer_kernel(
+    fs, slots,
+    stream_ref, mixed_ref, out_ref, gain_ref, up_ref, down_ref, result_ref,
+    mixw, gains, wo, wup, wdn, rows, acts, kept, send_c, got_c, send_y, got_y, send_z, got_z,
+    send_sem, recv_sem, local_sem,
+):
+    f32, bf16 = jnp.float32, jnp.bfloat16
+    g, i, j = lax.axis_index("grp"), lax.axis_index("fs"), lax.axis_index("tp")
+    y, c = j // 2, j % 2
+    jc = y * 2 + (1 - c)
+    jy = (1 - y) * 2 + c
+    jd = (1 - y) * 2 + (1 - c)
+    half, width = wo.shape[2], wo.shape[3]
+    order = [s for s in (2, 1, 3) if s < fs] if fs == 4 else list(range(1, fs))
+
+    core, across, diag, twin = (g, i, jc), (g, i, jy), (g, i, jd), (1 - g, i, j)
+
+    def ahead(s):
+        return lax.rem(i + s, fs)
+
+    def behind(s):
+        return lax.rem(i + fs - s, fs)
+
+    def slice_of(s):
+        return (g, ahead(s), j)
+
+    sent = []
+
+    def copy(name, k, src, dst, target):
+        n = slots[name] + k
+        return pltpu.make_async_remote_copy(
+            src_ref=src, dst_ref=dst, send_sem=send_sem.at[n], recv_sem=recv_sem.at[n],
+            device_id=target, device_id_type=MESH,
+        )
+
+    def send(name, k, src, dst, target):
+        made = copy(name, k, src, dst, target)
+        made.start()
+        sent.append(made)
+
+    def arrive(name, k, dst, target):
+        copy(name, k, dst, dst, target).wait_recv()
+
+    barrier = pltpu.get_barrier_semaphore()
+    greeted = [core, across, diag, twin] + [slice_of(s) for s in order]
+    for device in greeted:
+        pl.semaphore_signal(barrier, inc=1, device_id=device, device_id_type=MESH)
+
+    local = []
+
+    def keep(src, dst):
+        made = pltpu.make_async_copy(src, dst, local_sem.at[len(local)])
+        made.start()
+        local.append(made)
+
+    def up_piece(owner, part):
+        return up_ref.at[pl.ds(part * half, half), pl.ds(pl.multiple_of(owner * width, width), width)]
+
+    def down_piece(owner, part):
+        return down_ref.at[pl.ds(owner * 2 * half + part * half, half), :]
+
+    for part in range(2):
+        keep(out_ref.at[pl.ds(part * half, half), :], wo.at[i, part])
+        keep(up_piece(i, part), wup.at[i, part])
+        keep(down_piece(i, part), wdn.at[i, part])
+    keep(mixed_ref, mixw.at[j])
+    keep(gain_ref, gains.at[j])
+    pl.semaphore_wait(barrier, len(greeted))
+
+    send("mixed", 0, mixed_ref, mixw.at[j], across)
+    send("mixed", 1, mixed_ref, mixw.at[j], core)
+    for s in order:
+        send("out_z", s, out_ref.at[pl.ds(g * half, half), :], wo.at[i, g], slice_of(s))
+    send("gain", 0, gain_ref, gains.at[j], across)
+    send("gain", 1, gain_ref, gains.at[j], core)
+    send("gain", 2, gain_ref, gains.at[j], diag)
+    for s in order:
+        send("up_z", s, up_piece(ahead(s), g), wup.at[i, g], slice_of(s))
+
+    arrive("mixed", 0, mixw.at[jy], across)
+    send("mixed", 2, mixw.at[jy], mixw.at[jy], core)
+    for s in order:
+        b = behind(s)
+        arrive("out_z", s, wo.at[b, g], slice_of(s))
+        send("out_x", s, wo.at[b, g], wo.at[b, g], twin)
+    arrive("mixed", 1, mixw.at[jc], core)
+    arrive("mixed", 2, mixw.at[jd], core)
+    for made in local:
+        made.wait()
+
+    def whole(ref, k):
+        return ref[k].reshape(2 * half, width)
+
+    total = stream_ref[...].astype(f32) + jnp.dot(mixw[i], whole(wo, i), preferred_element_type=f32)
+    for s in order:
+        b = behind(s)
+        arrive("out_x", s, wo.at[b, 1 - g], twin)
+        total += jnp.dot(mixw[b], whole(wo, b), preferred_element_type=f32)
+    rows[j, i] = total.astype(bf16)
+
+    for s in order:
+        send("rows_z", s, rows.at[j, i], rows.at[j, i], slice_of(s))
+    send("rows_y", 0, rows.at[j, i], rows.at[j, i], across)
+    send("rows_c", 0, rows.at[j, i], rows.at[j, i], core)
+    for s in order:
+        send("down_z", s, down_piece(ahead(s), g), wdn.at[i, g], slice_of(s))
+
+    for s in order:
+        b = behind(s)
+        arrive("up_z", s, wup.at[b, g], slice_of(s))
+        send("up_x", s, wup.at[b, g], wup.at[b, g], twin)
+    arrive("rows_y", 0, rows.at[jy, i], across)
+    send("rows_d", 0, rows.at[jy, i], rows.at[jy, i], core)
+    for s in order:
+        b = behind(s)
+        arrive("rows_z", s, rows.at[j, b], slice_of(s))
+        send("rows_y", s, rows.at[j, b], rows.at[j, b], across)
+        send("rows_c", s, rows.at[j, b], rows.at[j, b], core)
+    arrive("gain", 0, gains.at[jy], across)
+    arrive("gain", 1, gains.at[jc], core)
+    arrive("gain", 2, gains.at[jd], diag)
+    for s in order:
+        arrive("up_x", s, wup.at[behind(s), 1 - g], twin)
+
+    def hidden(t):
+        wide = [rows[k, t].astype(f32) for k in range(rows.shape[0])]
+        energy = sum(jnp.sum(w * w, axis=1, keepdims=True) for w in wide)
+        scale = lax.rsqrt(energy * (1.0 / (len(wide) * width)) + epsilon)
+        up = None
+        for k, w in enumerate(wide):
+            normed = (w * scale * gains[k].astype(f32)).astype(bf16)
+            term = jnp.dot(normed, whole(wup, k), preferred_element_type=f32)
+            up = term if up is None else up + term
+        return jnp.square(jnp.maximum(up, 0.0)).astype(bf16)
+
+    for s in [0] + order:
+        b = behind(s)
+        if s > 0:
+            arrive("rows_y", s, rows.at[jy, b], across)
+            send("rows_d", s, rows.at[jy, b], rows.at[jy, b], core)
+        arrive("rows_c", s, rows.at[jc, b], core)
+        arrive("rows_d", s, rows.at[jd, b], core)
+        acts[b] = hidden(b)
+
+    for s in order:
+        b = behind(s)
+        arrive("down_z", s, wdn.at[b, g], slice_of(s))
+        send("down_x", s, wdn.at[b, g], wdn.at[b, g], twin)
+    for s in order:
+        arrive("down_x", s, wdn.at[behind(s), 1 - g], twin)
+
+    def share(t, column):
+        return jnp.dot(acts[t], whole(wdn, column), preferred_element_type=f32)
+
+    last = order + [0]
+    for s in last:
+        t = ahead(s)
+        send_c[t, 0] = share(t, jc).astype(bf16)
+        send_c[t, 1] = share(t, jd).astype(bf16)
+        send("sum_c", s, send_c.at[t], got_c.at[t], core)
+    for s in last:
+        t = ahead(s)
+        far = share(t, jy)
+        kept[t] = share(t, j)
+        arrive("sum_c", s, got_c.at[t], core)
+        send_y[t] = (far + got_c[t, 1].astype(f32)).astype(bf16)
+        send("sum_y", s, send_y.at[t], got_y.at[t], across)
+    for s in order:
+        t = ahead(s)
+        arrive("sum_y", s, got_y.at[t], across)
+        send_z[t] = (kept[t] + got_c[t, 0].astype(f32) + got_y[t].astype(f32)).astype(bf16)
+        send("sum_z", s, send_z.at[t], got_z.at[i], slice_of(s))
+    arrive("sum_y", 0, got_y.at[i], across)
+    branch = kept[i] + got_c[i, 0].astype(f32) + got_y[i].astype(f32)
+    for s in order:
+        b = behind(s)
+        arrive("sum_z", s, got_z.at[b], slice_of(s))
+        branch += got_z[b].astype(f32)
+    result_ref[...] = (rows[j, i].astype(f32) + branch).astype(bf16)
+    for made in sent:
+        made.wait_send()
+
+
+def kernel_body(fs, tp, stream, mixed, out_weight, norm_gain, up_weight, down_weight):
+    tokens, width = stream.shape
+    half = out_weight.shape[0] // 2
+    slots, count = slot_table(fs)
+    vmem, anywhere = pl.BlockSpec(memory_space=pltpu.VMEM), pl.BlockSpec(memory_space=pl.ANY)
+    weights = pltpu.VMEM((fs, 2, half, width), jnp.bfloat16)
+    blocks = pltpu.VMEM((fs, tokens, width), jnp.bfloat16)
+    pairs = pltpu.VMEM((fs, 2, tokens, width), jnp.bfloat16)
+    return pl.pallas_call(
+        functools.partial(layer_kernel, fs, slots),
+        out_shape=jax.ShapeDtypeStruct((tokens, width), jnp.bfloat16),
+        in_specs=[vmem, vmem, anywhere, vmem, anywhere, anywhere],
+        out_specs=vmem,
+        scratch_shapes=[
+            pltpu.VMEM((tp, tokens, width), jnp.bfloat16),
+            pltpu.VMEM((tp, 1, width), jnp.bfloat16),
+            weights, weights, weights,
+            pltpu.VMEM((tp, fs, tokens, width), jnp.bfloat16),
+            blocks,
+            pltpu.VMEM((fs, tokens, width), jnp.float32),
+            pairs, pairs, blocks, blocks, blocks, blocks,
+            pltpu.SemaphoreType.DMA((count,)),
+            pltpu.SemaphoreType.DMA((count,)),
+            pltpu.SemaphoreType.DMA((8,)),
+        ],
+        compiler_params=pltpu.CompilerParams(
+            collective_id=0, has_side_effects=True, vmem_limit_bytes=56 * 1024 * 1024
+        ),
+    )(stream, mixed, out_weight, norm_gain.reshape(1, width), up_weight, down_weight)
+
+
 def solution(mesh):
     placed = (
         P(("grp", "fs"), "tp"),
@@ -72,7 +305,11 @@
         tokens = stream.shape[0] // mesh.shape["grp"]
         moved_weights = 2 * width * hidden // tp
         moved_rows = 2 * tokens * width + 2 * width * hidden // (tp * fs)
+        aligned = fs == tp == 4 and (width // tp) % 256 == 0 and (tokens // fs) % 16 == 0
+        aligned = aligned and hidden == tp * width
         body = spread_body if moved_rows < moved_weights else gathered_body
+        if aligned and moved_rows < moved_weights:
+            body = functools.partial(kernel_body, fs, tp)
         return sharded(body)(stream, mixed, out_weight, norm_gain, up_weight, down_weight)
 
     def sharded(body):

time: 299 us -> 157 us (0.53)
  waiting for transfers between devices: 241 us -> 0 us
  Pallas kernels: 0 us -> 153 us
  between operations: 13.5 us -> 0.01 us
  matrix products: 12.7 us -> 0 us
  starting transfers between devices: 8.42 us -> 0 us
  local copies, waits for them, and re-layouts: 10.6 us -> 2.93 us
  blocking collectives: 6.6 us -> 0 us
  other arithmetic: 4.95 us -> 0 us
    pallas_call x0 -> x1, Pallas kernels: none -> 153 us  [kernel_body(): pl.pallas_call(functools.partial(layer_kernel, fs, slots), out_shape=jax....]
    all_gather x4 -> x0, waiting for transfers between devices: 108 us -> none  [the longest x1 46.7 us: spread_body(): out_full = lax.all_gather(out_weight, 'fs', axis=0, tiled=True)]
    reduce_scatter x2 -> x0, waiting for transfers between devices: 73.3 us -> none  [the longest x1 44.1 us: spread_body(): columns = lax.psum_scatter(partials, 'tp', scatter_dimension=1, tiled=True)]
    all_to_all x2 -> x0, waiting for transfers between devices: 57.8 us -> none  [the longest x1 38.7 us: spread_body(): lax.all_to_all(up_weight, 'fs', split_axis=1, concat_axis=0, tiled=True)]
    dot_general x2 -> x0, matrix products: 12.7 us -> none  [the longest x1 9.4 us: spread_body(): jnp.dot(activated, down_mine, preferred_element_type=jnp.float32)]
    all_to_all x2 -> x0, starting transfers between devices: 8.21 us -> none  [the longest x1 4.59 us: spread_body(): lax.all_to_all(up_weight, 'fs', split_axis=1, concat_axis=0, tiled=True)]
    all_to_all x2 -> x0, local copies, waits for them, and re-layouts: 6.6 us -> none  [the longest x1 4.2 us: spread_body(): lax.all_to_all(up_weight, 'fs', split_axis=1, concat_axis=0, tiled=True)]
    all_gather x1 -> x0, blocking collectives: 6.6 us -> none  [spread_body(): lax.all_gather(norm_gain, 'tp', axis=0, tiled=True).astype(jnp.float32)]
  transfers between devices with their start and end apart: 8 -> 0, of which waited for: 7 -> 0; matrix products, arithmetic and copies ran while one was open for 4% -> 0% of each run, Pallas kernels for 0% -> 0%
where the time goes in v2:
time: 157 us; the launch traced here: 156 us
  Pallas kernels  153 us (97%)
  local copies, waits for them, and re-layouts  2.93 us (2%)
    pallas_call x1, Pallas kernels, kernel_body(): pl.pallas_call(functools.partial(layer_kernel, fs, slots), out_shape=jax....  153 us

profile of v2, /device:TPU:1, one launch (start us, length us, event | category | flops | bytes accessed | tf_op | source)
XLA Modules:
  0.0 155.5 jit_solution(10828767934125579788)
XLA Ops:
  0.0 1.3 reshape.3.gain_ref
  1.3 152.6 %shard_map.64 = bf16[256,512]{1,0:T(8,128)(2,1)} custom-call(bf16[256,512]{1,0:T(8,128)(2,1)} %stream_ref.1, bf16[256,512]{1,0:T(8,128)(2,1)} %mixed_ref.1, bf16[512,512]{1,0:T(8,128)(2,1)} %out_ref.1, bf16[1,512]{1,0:T(2,128)(2,1)} %reshape.3.gain_ref, bf16[512,2048]{1,0:T(8,128)(2,1)} %up_ref.1, bf16[2048,512]{1,0:T(8,128)(2,1)} %down_ref.1), custom_call_target="tpu_custom_call" | custom-call | tf_op jit(solution)/shard_map/pallas_call | solution.py:269
  153.8 1.7 %copy.8 = bf16[256,512]{1,0:T(8,128)(2,1)} copy(bf16[256,512]{1,0:T(8,128)(2,1)} %shard_map.64) | data formatting | bytes 524288

commit v3 on v2

--- a/solution.py
+++ b/solution.py
@@ -65,9 +65,11 @@
 
 def slot_table(fs):
     table, count = {}, 0
+    hops = 2 * (fs - 1)
     sizes = dict(
-        mixed=3, gain=3, out_z=fs, out_x=fs, up_z=fs, up_x=fs, down_z=fs, down_x=fs,
-        rows_z=fs, rows_y=fs, rows_c=fs, rows_d=fs, sum_c=fs, sum_y=fs, sum_z=fs, own=fs,
+        mixed=3, gain=3, out_z=hops, out_x=hops, up_z=fs, up_x=fs, down_z=fs, down_x=fs,
+        rows_z=hops, rows_y=hops + 1, rows_c=hops + 1, rows_d=hops + 1,
+        sum_c=fs * fs, sum_y=fs, sum_z=fs,
     )
     for name, size in sizes.items():
         table[name] = count
@@ -78,7 +80,7 @@
 def layer_kernel(
     fs, slots,
     stream_ref, mixed_ref, out_ref, gain_ref, up_ref, down_ref, result_ref,
-    mixw, gains, wo, wup, wdn, rows, acts, kept, send_c, got_c, send_y, got_y, send_z, got_z,
+    mixw, gains, wo, wup, wdn, rows, acts, kept, mine, send_c, got_c, send_y, got_y, send_z, got_z,
     send_sem, recv_sem, local_sem,
 ):
     f32, bf16 = jnp.float32, jnp.bfloat16
@@ -110,10 +112,45 @@
             device_id=target, device_id_type=MESH,
         )
 
-    def send(name, k, src, dst, target):
+    def send(name, k, src, dst, target, given=None):
         made = copy(name, k, src, dst, target)
         made.start()
-        sent.append(made)
+        sent.append((made, None) if given is None else ((name, k), given))
+
+    both = jnp.logical_and
+
+    hops = [(side, d) for d in range(1, fs) for side in range(2)]
+
+    def hop(side, d):
+        return side * (fs - 1) + d - 1
+
+    def neighbour(side):
+        return slice_of(1) if side == 0 else slice_of(fs - 1)
+
+    def onward(side):
+        return i < fs - 1 if side == 0 else i > 0
+
+    def start_relay(name, src, dst):
+        for side in range(2):
+            @pl.when(onward(side))
+            def _():
+                send(name, hop(side, 1), src, dst, neighbour(side), lambda side=side: onward(side))
+
+    def take_relay(name, side, d, block_of, then):
+        has = i >= d if side == 0 else i + d < fs
+        b = i - d if side == 0 else i + d
+
+        @pl.when(has)
+        def _():
+            arrive(name, hop(side, d), block_of(b), neighbour(1 - side))
+            if d < fs - 1:
+                @pl.when(onward(side))
+                def _():
+                    send(
+                        name, hop(side, d + 1), block_of(b), block_of(b), neighbour(side),
+                        lambda: both(has, onward(side)),
+                    )
+            then(b, hop(side, d), lambda: has)
 
     def arrive(name, k, dst, target):
         copy(name, k, dst, dst, target).wait_recv()
@@ -146,20 +183,24 @@
 
     send("mixed", 0, mixed_ref, mixw.at[j], across)
     send("mixed", 1, mixed_ref, mixw.at[j], core)
-    for s in order:
-        send("out_z", s, out_ref.at[pl.ds(g * half, half), :], wo.at[i, g], slice_of(s))
+    start_relay("out_z", out_ref.at[pl.ds(g * half, half), :], wo.at[i, g])
     send("gain", 0, gain_ref, gains.at[j], across)
     send("gain", 1, gain_ref, gains.at[j], core)
     send("gain", 2, gain_ref, gains.at[j], diag)
-    for s in order:
-        send("up_z", s, up_piece(ahead(s), g), wup.at[i, g], slice_of(s))
-
+
+    def out_block(b):
+        return wo.at[b, g]
+
+    def out_cross(b, n, has):
+        send("out_x", n, out_block(b), out_block(b), twin, has)
+
+    for side, d in hops:
+        if d == fs - 1 and side == 0:
+            for s in order:
+                send("up_z", s, up_piece(ahead(s), g), wup.at[i, g], slice_of(s))
+        take_relay("out_z", side, d, out_block, out_cross)
     arrive("mixed", 0, mixw.at[jy], across)
     send("mixed", 2, mixw.at[jy], mixw.at[jy], core)
-    for s in order:
-        b = behind(s)
-        arrive("out_z", s, wo.at[b, g], slice_of(s))
-        send("out_x", s, wo.at[b, g], wo.at[b, g], twin)
     arrive("mixed", 1, mixw.at[jc], core)
     arrive("mixed", 2, mixw.at[jd], core)
     for made in local:
@@ -168,19 +209,22 @@
     def whole(ref, k):
         return ref[k].reshape(2 * half, width)
 
-    total = stream_ref[...].astype(f32) + jnp.dot(mixw[i], whole(wo, i), preferred_element_type=f32)
-    for s in order:
-        b = behind(s)
-        arrive("out_x", s, wo.at[b, 1 - g], twin)
-        total += jnp.dot(mixw[b], whole(wo, b), preferred_element_type=f32)
+    for side, d in hops:
+        has = i >= d if side == 0 else i + d < fs
+        b = i - d if side == 0 else i + d
+
+        @pl.when(has)
+        def _():
+            arrive("out_x", hop(side, d), wo.at[b, 1 - g], twin)
+
+    total = stream_ref[...].astype(f32)
+    for k in range(fs):
+        total += jnp.dot(mixw[k], whole(wo, k), preferred_element_type=f32)
     rows[j, i] = total.astype(bf16)
 
-    for s in order:
-        send("rows_z", s, rows.at[j, i], rows.at[j, i], slice_of(s))
+    start_relay("rows_z", rows.at[j, i], rows.at[j, i])
     send("rows_y", 0, rows.at[j, i], rows.at[j, i], across)
     send("rows_c", 0, rows.at[j, i], rows.at[j, i], core)
-    for s in order:
-        send("down_z", s, down_piece(ahead(s), g), wdn.at[i, g], slice_of(s))
 
     for s in order:
         b = behind(s)
@@ -188,11 +232,19 @@
         send("up_x", s, wup.at[b, g], wup.at[b, g], twin)
     arrive("rows_y", 0, rows.at[jy, i], across)
     send("rows_d", 0, rows.at[jy, i], rows.at[jy, i], core)
-    for s in order:
-        b = behind(s)
-        arrive("rows_z", s, rows.at[j, b], slice_of(s))
-        send("rows_y", s, rows.at[j, b], rows.at[j, b], across)
-        send("rows_c", s, rows.at[j, b], rows.at[j, b], core)
+
+    def rows_block(b):
+        return rows.at[j, b]
+
+    def rows_cross(b, n, has):
+        send("rows_y", n + 1, rows_block(b), rows_block(b), across, has)
+        send("rows_c", n + 1, rows_block(b), rows_block(b), core, has)
+
+    for side, d in hops:
+        if d == fs - 1 and side == 0:
+            for s in order:
+                send("down_z", s, down_piece(ahead(s), g), wdn.at[i, g], slice_of(s))
+        take_relay("rows_z", side, d, rows_block, rows_cross)
     arrive("gain", 0, gains.at[jy], across)
     arrive("gain", 1, gains.at[jc], core)
     arrive("gain", 2, gains.at[jd], diag)
@@ -210,52 +262,76 @@
             up = term if up is None else up + term
         return jnp.square(jnp.maximum(up, 0.0)).astype(bf16)
 
-    for s in [0] + order:
-        b = behind(s)
+    arrive("rows_c", 0, rows.at[jc, i], core)
+    arrive("rows_d", 0, rows.at[jd, i], core)
+    acts[i] = hidden(i)
+    for side, d in hops:
+        has = i >= d if side == 0 else i + d < fs
+        b = i - d if side == 0 else i + d
+        n = hop(side, d) + 1
+
+        @pl.when(has)
+        def _():
+            arrive("rows_y", n, rows.at[jy, b], across)
+            send("rows_d", n, rows.at[jy, b], rows.at[jy, b], core, lambda has=has: has)
+            arrive("rows_c", n, rows.at[jc, b], core)
+            arrive("rows_d", n, rows.at[jd, b], core)
+            acts[b] = hidden(b)
+
+    last = order + [0]
+
+    def column(n, k):
+        ck, yk = k % 2, k // 2
+        w = whole(wdn, k)
+
+        @pl.when(ck != c)
+        def _():
+            for s in last:
+                t = ahead(s)
+                send_c[yk, t] = jnp.dot(acts[t], w, preferred_element_type=f32).astype(bf16)
+                send("sum_c", n * fs + s, send_c.at[yk, t], got_c.at[yk, t], core, lambda: ck != c)
+
+        @pl.when(ck == c)
+        def _():
+            for s in last:
+                t = ahead(s)
+                part = jnp.dot(acts[t], w, preferred_element_type=f32)
+                arrive("sum_c", n * fs + s, got_c.at[yk, t], core)
+                kept[t] = part + got_c[yk, t].astype(f32)
+
+                @pl.when(yk != y)
+                def _():
+                    send_y[t] = kept[t].astype(bf16)
+                    send("sum_y", s, send_y.at[t], got_y.at[t], across, lambda: both(ck == c, yk != y))
+
+                @pl.when(yk == y)
+                def _():
+                    mine[t] = kept[t]
+
+    for n, s in enumerate([0] + order):
         if s > 0:
-            arrive("rows_y", s, rows.at[jy, b], across)
-            send("rows_d", s, rows.at[jy, b], rows.at[jy, b], core)
-        arrive("rows_c", s, rows.at[jc, b], core)
-        arrive("rows_d", s, rows.at[jd, b], core)
-        acts[b] = hidden(b)
-
-    for s in order:
-        b = behind(s)
-        arrive("down_z", s, wdn.at[b, g], slice_of(s))
-        send("down_x", s, wdn.at[b, g], wdn.at[b, g], twin)
-    for s in order:
-        arrive("down_x", s, wdn.at[behind(s), 1 - g], twin)
-
-    def share(t, column):
-        return jnp.dot(acts[t], whole(wdn, column), preferred_element_type=f32)
-
-    last = order + [0]
-    for s in last:
-        t = ahead(s)
-        send_c[t, 0] = share(t, jc).astype(bf16)
-        send_c[t, 1] = share(t, jd).astype(bf16)
-        send("sum_c", s, send_c.at[t], got_c.at[t], core)
-    for s in last:
-        t = ahead(s)
-        far = share(t, jy)
-        kept[t] = share(t, j)
-        arrive("sum_c", s, got_c.at[t], core)
-        send_y[t] = (far + got_c[t, 1].astype(f32)).astype(bf16)
-        send("sum_y", s, send_y.at[t], got_y.at[t], across)
+            arrive("down_z", s, wdn.at[behind(s), g], slice_of(s))
+            send("down_x", s, wdn.at[behind(s), g], wdn.at[behind(s), g], twin)
+            arrive("down_x", s, wdn.at[behind(s), 1 - g], twin)
+        column(n, behind(s))
     for s in order:
         t = ahead(s)
         arrive("sum_y", s, got_y.at[t], across)
-        send_z[t] = (kept[t] + got_c[t, 0].astype(f32) + got_y[t].astype(f32)).astype(bf16)
+        send_z[t] = (mine[t] + got_y[t].astype(f32)).astype(bf16)
         send("sum_z", s, send_z.at[t], got_z.at[i], slice_of(s))
     arrive("sum_y", 0, got_y.at[i], across)
-    branch = kept[i] + got_c[i, 0].astype(f32) + got_y[i].astype(f32)
+    branch = mine[i] + got_y[i].astype(f32)
     for s in order:
         b = behind(s)
         arrive("sum_z", s, got_z.at[b], slice_of(s))
         branch += got_z[b].astype(f32)
     result_ref[...] = (rows[j, i].astype(f32) + branch).astype(bf16)
-    for made in sent:
-        made.wait_send()
+    for made, given in sent:
+        if given is None:
+            made.wait_send()
+        else:
+            block = wo.at[0, 0] if made[0].startswith("out") else rows.at[0, 0]
+            pl.when(given())(copy(*made, block, block, core).wait_send)
 
 
 def kernel_body(fs, tp, stream, mixed, out_weight, norm_gain, up_weight, down_weight):
@@ -265,7 +341,8 @@
     vmem, anywhere = pl.BlockSpec(memory_space=pltpu.VMEM), pl.BlockSpec(memory_space=pl.ANY)
     weights = pltpu.VMEM((fs, 2, half, width), jnp.bfloat16)
     blocks = pltpu.VMEM((fs, tokens, width), jnp.bfloat16)
-    pairs = pltpu.VMEM((fs, 2, tokens, width), jnp.bfloat16)
+    columns = pltpu.VMEM((2, fs, tokens, width), jnp.bfloat16)
+    sums = pltpu.VMEM((fs, tokens, width), jnp.float32)
     return pl.pallas_call(
         functools.partial(layer_kernel, fs, slots),
         out_shape=jax.ShapeDtypeStruct((tokens, width), jnp.bfloat16),
@@ -277,8 +354,8 @@
             weights, weights, weights,
             pltpu.VMEM((tp, fs, tokens, width), jnp.bfloat16),
             blocks,
-            pltpu.VMEM((fs, tokens, width), jnp.float32),
-            pairs, pairs, blocks, blocks, blocks, blocks,
+            sums, sums,
+            columns, columns, blocks, blocks, blocks, blocks,
             pltpu.SemaphoreType.DMA((count,)),
             pltpu.SemaphoreType.DMA((count,)),
             pltpu.SemaphoreType.DMA((8,)),

time: 157 us -> 133 us (0.85); the launches traced: 156 us -> 133 us
  Pallas kernels: 153 us -> 130 us
    pallas_call x1, Pallas kernels: 153 us -> 130 us  [kernel_body(): pl.pallas_call(functools.partial(layer_kernel, fs, slots), out_shape=jax....]
where the time goes in v3:
time: 133 us
  Pallas kernels  130 us (98%)
  local copies, waits for them, and re-layouts  2.93 us (2%)
    pallas_call x1, Pallas kernels, kernel_body(): pl.pallas_call(functools.partial(layer_kernel, fs, slots), out_shape=jax....  130 us

profile of v3, /device:TPU:1, one launch (start us, length us, event | category | flops | bytes accessed | tf_op | source)
XLA Modules:
  0.0 133.3 jit_solution(15664543092414921360)
XLA Ops:
  0.0 1.3 reshape.3.gain_ref
  1.3 130.4 %shard_map.64 = bf16[256,512]{1,0:T(8,128)(2,1)} custom-call(bf16[256,512]{1,0:T(8,128)(2,1)} %stream_ref.1, bf16[256,512]{1,0:T(8,128)(2,1)} %mixed_ref.1, bf16[512,512]{1,0:T(8,128)(2,1)} %out_ref.1, bf16[1,512]{1,0:T(2,128)(2,1)} %reshape.3.gain_ref, bf16[512,2048]{1,0:T(8,128)(2,1)} %up_ref.1, bf16[2048,512]{1,0:T(8,128)(2,1)} %down_ref.1), custom_call_target="tpu_custom_call" | custom-call | tf_op jit(solution)/shard_map/pallas_call | solution.py:346
  131.6 1.7 %copy.8 = bf16[256,512]{1,0:T(8,128)(2,1)} copy(bf16[256,512]{1,0:T(8,128)(2,1)} %shard_map.64) | data formatting | bytes 524288

commit v4 on v3

--- a/solution.py
+++ b/solution.py
@@ -262,6 +262,10 @@
             up = term if up is None else up + term
         return jnp.square(jnp.maximum(up, 0.0)).astype(bf16)
 
+    def cross_down(s):
+        arrive("down_z", s, wdn.at[behind(s), g], slice_of(s))
+        send("down_x", s, wdn.at[behind(s), g], wdn.at[behind(s), g], twin)
+
     arrive("rows_c", 0, rows.at[jc, i], core)
     arrive("rows_d", 0, rows.at[jd, i], core)
     acts[i] = hidden(i)
@@ -269,6 +273,8 @@
         has = i >= d if side == 0 else i + d < fs
         b = i - d if side == 0 else i + d
         n = hop(side, d) + 1
+        if d == fs - 1 and side == 0:
+            cross_down(order[0])
 
         @pl.when(has)
         def _():
@@ -308,17 +314,25 @@
                 def _():
                     mine[t] = kept[t]
 
+    def owned(given):
+        @pl.when(given)
+        def _():
+            for s in order:
+                t = ahead(s)
+                arrive("sum_y", s, got_y.at[t], across)
+                send_z[t] = (mine[t] + got_y[t].astype(f32)).astype(bf16)
+                send("sum_z", s, send_z.at[t], got_z.at[i], slice_of(s), lambda: given)
+
+    early = jnp.logical_or(behind(0) == j, behind(order[0]) == j)
     for n, s in enumerate([0] + order):
+        if 0 < n < len(order):
+            cross_down(order[n])
         if s > 0:
-            arrive("down_z", s, wdn.at[behind(s), g], slice_of(s))
-            send("down_x", s, wdn.at[behind(s), g], wdn.at[behind(s), g], twin)
             arrive("down_x", s, wdn.at[behind(s), 1 - g], twin)
         column(n, behind(s))
-    for s in order:
-        t = ahead(s)
-        arrive("sum_y", s, got_y.at[t], across)
-        send_z[t] = (mine[t] + got_y[t].astype(f32)).astype(bf16)
-        send("sum_z", s, send_z.at[t], got_z.at[i], slice_of(s))
+        if n == len(order) - 1:
+            owned(early)
+    owned(jnp.logical_not(early))
     arrive("sum_y", 0, got_y.at[i], across)
     branch = mine[i] + got_y[i].astype(f32)
     for s in order:

time: 133 us -> 124 us (0.932)
  Pallas kernels: 130 us -> 121 us
    pallas_call x1, Pallas kernels: 130 us -> 121 us  [kernel_body(): pl.pallas_call(functools.partial(layer_kernel, fs, slots), out_shape=jax....]
where the time goes in v4:
time: 124 us
  Pallas kernels  121 us (98%)
  local copies, waits for them, and re-layouts  2.93 us (2%)
    pallas_call x1, Pallas kernels, kernel_body(): pl.pallas_call(functools.partial(layer_kernel, fs, slots), out_shape=jax....  121 us

profile of v4, /device:TPU:1, one launch (start us, length us, event | category | flops | bytes accessed | tf_op | source)
XLA Modules:
  0.0 124.3 jit_solution(1406589503927454738)
XLA Ops:
  0.0 1.3 %reshape.3.gain_ref = bf16[1,512]{1,0:T(2,128)(2,1)} reshape(bf16[512]{0:T(512)(128)(2,1)} %param.9) | data formatting | bytes 2048 | tf_op jit(solution)/shard_map/reshape | solution.py:380
  1.3 121.4 %shard_map.64 = bf16[256,512]{1,0:T(8,128)(2,1)} custom-call(bf16[256,512]{1,0:T(8,128)(2,1)} %stream_ref.1, bf16[256,512]{1,0:T(8,128)(2,1)} %mixed_ref.1, bf16[512,512]{1,0:T(8,128)(2,1)} %out_ref.1, bf16[1,512]{1,0:T(2,128)(2,1)} %reshape.3.gain_ref, bf16[512,2048]{1,0:T(8,128)(2,1)} %up_ref.1, bf16[2048,512]{1,0:T(8,128)(2,1)} %down_ref.1), custom_call_target="tpu_custom_call" | custom-call | tf_op jit(solution)/shard_map/pallas_call | solution.py:360
  122.6 1.7 %copy.8 = bf16[256,512]{1,0:T(8,128)(2,1)} copy(bf16[256,512]{1,0:T(8,128)(2,1)} %shard_map.64) | data formatting | bytes 524288

commit v5 on v4

--- a/solution.py
+++ b/solution.py
@@ -195,8 +195,8 @@
         send("out_x", n, out_block(b), out_block(b), twin, has)
 
     for side, d in hops:
-        if d == fs - 1 and side == 0:
-            for s in order:
+        if d >= fs - 2 and side == 0:
+            for s in order[1:] if d == fs - 1 else order[:1]:
                 send("up_z", s, up_piece(ahead(s), g), wup.at[i, g], slice_of(s))
         take_relay("out_z", side, d, out_block, out_cross)
     arrive("mixed", 0, mixw.at[jy], across)
@@ -241,8 +241,8 @@
         send("rows_c", n + 1, rows_block(b), rows_block(b), core, has)
 
     for side, d in hops:
-        if d == fs - 1 and side == 0:
-            for s in order:
+        if d >= fs - 2 and side == 0:
+            for s in order[1:] if d == fs - 1 else order[:1]:
                 send("down_z", s, down_piece(ahead(s), g), wdn.at[i, g], slice_of(s))
         take_relay("rows_z", side, d, rows_block, rows_cross)
     arrive("gain", 0, gains.at[jy], across)

time: 124 us -> 134 us (1.081); the launches traced: 124 us -> 133 us
  Pallas kernels: 121 us -> 130 us
    pallas_call x1, Pallas kernels: 121 us -> 130 us  [kernel_body(): pl.pallas_call(functools.partial(layer_kernel, fs, slots), out_shape=jax....]
where the time goes in v5:
time: 134 us; the launch traced here: 133 us
  Pallas kernels  130 us (97%)
  local copies, waits for them, and re-layouts  2.93 us (2%)
    pallas_call x1, Pallas kernels, kernel_body(): pl.pallas_call(functools.partial(layer_kernel, fs, slots), out_shape=jax....  130 us

profile of v5, /device:TPU:1, one launch (start us, length us, event | category | flops | bytes accessed | tf_op | source)
XLA Modules:
  0.0 132.8 jit_solution(2760305425721195891)
XLA Ops:
  0.0 1.3 reshape.3.gain_ref
  1.3 129.9 %shard_map.64 = bf16[256,512]{1,0:T(8,128)(2,1)} custom-call(bf16[256,512]{1,0:T(8,128)(2,1)} %stream_ref.1, bf16[256,512]{1,0:T(8,128)(2,1)} %mixed_ref.1, bf16[512,512]{1,0:T(8,128)(2,1)} %out_ref.1, bf16[1,512]{1,0:T(2,128)(2,1)} %reshape.3.gain_ref, bf16[512,2048]{1,0:T(8,128)(2,1)} %up_ref.1, bf16[2048,512]{1,0:T(8,128)(2,1)} %down_ref.1), custom_call_target="tpu_custom_call" | custom-call | tf_op jit(solution)/shard_map/pallas_call | solution.py:360
  131.1 1.7 %copy.8 = bf16[256,512]{1,0:T(8,128)(2,1)} copy(bf16[256,512]{1,0:T(8,128)(2,1)} %shard_map.64) | data formatting | bytes 524288
